TPU v7x, 32 devices: a whole 2x2x4 slice. The times are simulated.
32 devices in a mesh: sp: 8 (over z, y), dp: 4 (over x, core).
Axes of the slice: x: 2, y: 2, z: 4, core: 2. Of those that a mesh axis runs over, the one named last changes fastest.
Arguments:
- queries: bfloat16 [4, 1024, 1024], P('dp', 'sp'), may hold values from -6 to 6
- keys: bfloat16 [4, 1024, 1024], P('dp', 'sp'), may hold values from -6 to 6
- values: bfloat16 [4, 1024, 2048], P('dp', 'sp'), may hold values from -6 to 6
- decay_in: bfloat16 [4, 1024, 16], P('dp', 'sp'), may hold values from -1 to 2048
- mix_in: bfloat16 [4, 1024, 16], P('dp', 'sp'), may hold values from -6 to 6
- rates: float32 [16], replicated, may hold values from 0 to 1, as said below
- head_gain: float32 [128], replicated, may hold values from 0.1 to 1.9
- out_weight: bfloat16 [2048, 2048], replicated, may hold values from -0.125 to 0.125
- residual: bfloat16 [4, 1024, 2048], P('dp', 'sp'), may hold values from -6 to 6
- mix_gain: float32 [2048], replicated, may hold values from 0.1 to 1.9
- ffn_gain: float32 [2048], replicated, may hold values from 0.1 to 1.9
- route: int32 [4, 1024, 2], P('dp', 'sp'), may hold values from 0 to 31, all different within a row; in each aligned block of 128 rows (0 to 127, 128 to 255, ..., all dimensions but the last counted through in order) at most 16 rows name the same one
- route_weight: float32 [4, 1024, 2], P('dp', 'sp'), may hold values from 0.1 to 1
- w_gate: bfloat16 [32, 2048, 512], P(('sp', 'dp')), may hold values from -0.125 to 0.125
- w_up: bfloat16 [32, 2048, 512], P(('sp', 'dp')), may hold values from -0.125 to 0.125
- w_down: bfloat16 [32, 512, 2048], P(('sp', 'dp')), may hold values from -0.25 to 0.25
- out_gain: float32 [2048], replicated, may hold values from 0.1 to 1.9
Outputs:
- mixed: bfloat16 [4, 1024, 2048], P('dp', 'sp')
Inputs may be any that keep to these rules, and one draw needn't show every extreme that they name: `route`: in the rows of one device no expert is named by more than 16 rows, and one is named by exactly 16; a row names 2 different experts. `rates`: Positive.
All inputs are finite; a program needn't handle non-finite values.
Results may differ from a plain program's by a relative error of at most 0.015.
Values may be sent and summed in bfloat16 or wider, within the bound.
A program may use at most 128 MiB of HBM per device.

v0:
```python
import functools

import jax
import jax.numpy as jnp
from jax import lax
from jax.experimental import pallas as pl
from jax.experimental.pallas import tpu as pltpu
from jax.sharding import PartitionSpec as P

DK = 64
DV = 128
TOPK = 2
BLOCK = 128
EPSILON = 1e-06
PRECISE = lax.Precision.HIGHEST
MESH = pl.DeviceIdType.MESH
VMEM = pl.BlockSpec(memory_space=pltpu.VMEM)
ANY = pl.BlockSpec(memory_space=pl.ANY)
HALF = jnp.bfloat16
NN = (((1,), (0,)), ((), ()))
NT = (((1,), (1,)), ((), ()))
TN = (((0,), (0,)), ((), ()))


def dot(a, b, dims=NN, precision=None):
    return lax.dot_general(a, b, dims, precision=precision, preferred_element_type=jnp.float32)


def unit_rows(x):
    return x * lax.rsqrt(jnp.sum(x * x, axis=-1, keepdims=True) + EPSILON)


def scale_rows(x, gain):
    return x * lax.rsqrt(jnp.mean(x * x, axis=-1, keepdims=True) + EPSILON) * gain


def pair_width(local_heads):
    return max(DV, local_heads * DK)


def block_kernel(groups, local_heads, q_ref, k_ref, v_ref, decay_ref, mix_ref, rates_ref, ab_ref, o_ref, qe_ref):
    length = q_ref.shape[0]
    heads = groups * local_heads
    rows = lax.broadcasted_iota(jnp.int32, (length, length), 0)
    cols = lax.broadcasted_iota(jnp.int32, (length, length), 1)
    lower = rows >= cols
    strict = rows > cols
    decay = decay_ref[...].astype(jnp.float32)
    softplus = jnp.maximum(decay, 0.0) + jnp.log1p(jnp.exp(-jnp.abs(decay)))
    log_decay = -rates_ref[...] * softplus
    beta = 1.0 / (1.0 + jnp.exp(-mix_ref[...].astype(jnp.float32)))
    running = dot(lower.astype(jnp.float32), log_decay, NN, PRECISE)
    spot_r = lax.broadcasted_iota(jnp.int32, (heads, heads), 0)
    spot_c = lax.broadcasted_iota(jnp.int32, (heads, heads), 1)
    running_t = dot((spot_r == spot_c).astype(jnp.float32), running, NT, PRECISE)
    grow = jnp.exp(running)
    total = running[length - 1 : length, :]
    shrink = jnp.exp(total - running)
    whole = jnp.exp(total)
    eye = (
        lax.broadcasted_iota(jnp.int32, (DK, DK), 0) == lax.broadcasted_iota(jnp.int32, (DK, DK), 1)
    ).astype(jnp.float32)
    scale = DK ** (-0.5)
    batch = 8 if heads % 8 == 0 else 1
    base = pair_width(local_heads)
    for first in range(0, heads, batch):
        own = range(first, first + batch)
        work = []
        for h in own:
            qn = unit_rows(q_ref[:, h * DK : (h + 1) * DK].astype(jnp.float32)).astype(HALF)
            kn = unit_rows(k_ref[:, h * DK : (h + 1) * DK].astype(jnp.float32)).astype(HALF)
            spread = running[:, h : h + 1] - running_t[h : h + 1, :]
            tile = jnp.where(lower, jnp.exp(jnp.where(lower, spread, 0.0)), 0.0)
            bet = beta[:, h : h + 1]
            strict_part = jnp.where(strict, dot(kn, kn, NT) * bet * tile, 0.0)
            scores = (dot(qn, kn, NT) * scale * tile).astype(HALF)
            work.append((qn, kn, strict_part, scores))
        size = 1
        inverses = [None] * batch
        while size < length:
            joins = (rows // (2 * size) == cols // (2 * size)) & ((rows // size) % 2 == 1) & ((cols // size) % 2 == 0)
            for i in range(batch):
                part = jnp.where(joins, work[i][2], 0.0)
                if size == 1:
                    inverses[i] = (rows == cols).astype(jnp.float32) - part
                else:
                    half = inverses[i].astype(HALF)
                    step = dot(part.astype(HALF), half)
                    inverses[i] = inverses[i] - dot(half, step.astype(HALF))
            size *= 2
        for i, h in enumerate(own):
            qn, kn, strict_part, scores = work[i]
            bet = beta[:, h : h + 1]
            key = kn.astype(jnp.float32)
            values = v_ref[:, h * DV : (h + 1) * DV].astype(jnp.float32) * bet
            inputs = jnp.concatenate([values, key * (bet * grow[:, h : h + 1])], axis=1)
            solved = dot(inverses[i].astype(HALF), inputs.astype(HALF))
            solved = solved.astype(HALF)
            seen = dot(scores, solved)
            kept = dot((key * shrink[:, h : h + 1]).astype(HALF), solved, TN)
            o_ref[:, h * DV : (h + 1) * DV] = seen[:, :DV]
            query = qn.astype(jnp.float32) * (scale * grow[:, h : h + 1])
            qe_ref[h] = (query - seen[:, DV:]).astype(HALF)
            owner, place = h // local_heads, h % local_heads
            ab_ref[owner, :, base + place * DV : base + (place + 1) * DV] = kept[:, :DV].astype(HALF)
            ab_ref[owner, :, place * DK : (place + 1) * DK] = (
                eye * whole[:, h : h + 1] - kept[:, DV:]
            ).astype(HALF)
            if local_heads * DK < base and place == local_heads - 1:
                ab_ref[owner, :, local_heads * DK : base] = jnp.zeros((DK, base - local_heads * DK), HALF)


def state_kernel(
    groups, local_heads,
    ab_ref, o_ref, qe_ref, hg_ref, w_hbm, res_ref, mg_ref, fg_ref,
    hidden_ref, normed_ref,
    ab_in, s_out, s_in, att, w_ref,
    w_sem, own_sem, send1, recv1, send2, recv2,
):
    me = lax.axis_index("sp")
    fetch = pltpu.make_async_copy(w_hbm, w_ref, w_sem)
    fetch.start()
    barrier = pltpu.get_barrier_semaphore()
    for step in range(1, groups):
        pl.semaphore_signal(barrier, inc=1, device_id={"sp": lax.rem(me + step, groups)}, device_id_type=MESH)
    pl.semaphore_wait(barrier, groups - 1)

    def first_copy(step):
        peer = lax.rem(me + step, groups)
        return pltpu.make_async_remote_copy(
            src_ref=ab_ref.at[peer], dst_ref=ab_in.at[me],
            send_sem=send1.at[step], recv_sem=recv1.at[step],
            device_id={"sp": peer}, device_id_type=MESH,
        )

    def second_copy(step):
        peer = lax.rem(me + step, groups)
        return pltpu.make_async_remote_copy(
            src_ref=s_out.at[peer], dst_ref=s_in.at[me],
            send_sem=send2.at[step], recv_sem=recv2.at[step],
            device_id={"sp": peer}, device_id_type=MESH,
        )

    for step in range(1, groups):
        first_copy(step).start()
    own = pltpu.make_async_copy(ab_ref.at[me], ab_in.at[me], own_sem)
    own.start()
    own.wait()
    for step in range(1, groups):
        first_copy(step).wait()
    base = pair_width(local_heads)
    states = [jnp.zeros((DK, DV), jnp.float32)] * local_heads
    for block in range(groups):
        for place in range(local_heads):
            half = states[place].astype(HALF)
            s_out[block, :, place * DV : (place + 1) * DV] = half
            if block < groups - 1:
                states[place] = (
                    dot(ab_in[block, :, place * DK : (place + 1) * DK], half)
                    + ab_in[block, :, base + place * DV : base + (place + 1) * DV].astype(jnp.float32)
                )
    for step in range(1, groups):
        second_copy(step).start()
    own = pltpu.make_async_copy(s_out.at[me], s_in.at[me], own_sem)
    own.start()
    own.wait()
    for step in range(1, groups):
        second_copy(step).wait()
    for h in range(groups * local_heads):
        owner, place = h // local_heads, h % local_heads
        state = s_in[owner, :, place * DV : (place + 1) * DV]
        out = o_ref[:, h * DV : (h + 1) * DV] + dot(qe_ref[h], state)
        att[:, h * DV : (h + 1) * DV] = scale_rows(out, hg_ref[...]).astype(HALF)
    fetch.wait()
    projected = dot(att[...], w_ref[...])
    hidden = (res_ref[...].astype(jnp.float32) + scale_rows(projected, mg_ref[...])).astype(HALF)
    hidden_ref[...] = hidden
    normed_ref[...] = scale_rows(hidden.astype(jnp.float32), fg_ref[...]).astype(HALF)


def expert_ffn(rows_in, gate_weight, up_weight, down_weight):
    gate = jnp.dot(rows_in, gate_weight, preferred_element_type=jnp.float32)
    upward = jnp.dot(rows_in, up_weight, preferred_element_type=jnp.float32)
    inner = (jax.nn.silu(gate) * upward).astype(jnp.bfloat16)
    return jnp.dot(inner, down_weight, preferred_element_type=jnp.float32).astype(jnp.bfloat16)


def local(
    queries,
    keys,
    values,
    decay_in,
    mix_in,
    rates,
    head_gain,
    out_weight,
    residual,
    mix_gain,
    ffn_gain,
    route,
    route_weight,
    w_gate,
    w_up,
    w_down,
    out_gain,
):
    groups = lax.axis_size("sp")
    tok_rows = queries.shape[1]
    head_count = rates.shape[0]
    local_heads = head_count // groups
    width = out_weight.shape[1]
    wide = pair_width(local_heads) + local_heads * DV
    pairs, partial, reads = pl.pallas_call(
        functools.partial(block_kernel, groups, local_heads),
        out_shape=(
            jax.ShapeDtypeStruct((groups, DK, wide), HALF),
            jax.ShapeDtypeStruct((tok_rows, head_count * DV), jnp.float32),
            jax.ShapeDtypeStruct((head_count, tok_rows, DK), HALF),
        ),
        in_specs=[VMEM] * 6,
        out_specs=(VMEM,) * 3,
        compiler_params=pltpu.CompilerParams(vmem_limit_bytes=40 << 20),
        name="block",
    )(queries[0], keys[0], values[0], decay_in[0], mix_in[0], rates.reshape(1, head_count))
    hidden_state, normed = pl.pallas_call(
        functools.partial(state_kernel, groups, local_heads),
        out_shape=(jax.ShapeDtypeStruct((tok_rows, width), HALF),) * 2,
        in_specs=[VMEM] * 4 + [ANY] + [VMEM] * 3,
        out_specs=(VMEM,) * 2,
        scratch_shapes=[
            pltpu.VMEM((groups, DK, wide), HALF),
            pltpu.VMEM((groups, DK, local_heads * DV), HALF),
            pltpu.VMEM((groups, DK, local_heads * DV), HALF),
            pltpu.VMEM((tok_rows, head_count * DV), HALF),
            pltpu.VMEM(out_weight.shape, HALF),
            pltpu.SemaphoreType.DMA,
            pltpu.SemaphoreType.DMA,
        ]
        + [pltpu.SemaphoreType.DMA((groups,))] * 4,
        compiler_params=pltpu.CompilerParams(
            collective_id=0, has_side_effects=True, vmem_limit_bytes=40 << 20
        ),
        name="state",
    )(
        pairs, partial, reads, head_gain.reshape(1, DV), out_weight, residual[0],
        mix_gain.reshape(1, width), ffn_gain.reshape(1, width),
    )
    experts = lax.axis_size("sp") * lax.axis_size("dp")
    capacity = max(2, 2 * tok_rows * TOPK // experts)
    route_ids = route.reshape(tok_rows * TOPK)
    matches = (route_ids[:, None] == jnp.arange(experts, dtype=jnp.int32)).astype(jnp.int32)
    slot_index = jnp.sum((jnp.cumsum(matches, axis=0) - 1) * matches, axis=-1)
    target = route_ids * capacity + slot_index
    copies = jnp.repeat(normed, TOPK, axis=0)
    outgoing = jnp.zeros((experts * capacity, width), jnp.bfloat16).at[target].set(copies)
    arrived_block = lax.all_to_all(
        outgoing.reshape(experts, capacity, width),
        ("sp", "dp"),
        split_axis=0,
        concat_axis=0,
        tiled=True,
    )
    block_shape = arrived_block.shape
    flat_rows = arrived_block.reshape(-1, block_shape[-1])
    served = expert_ffn(flat_rows, w_gate[0], w_up[0], w_down[0]).reshape(block_shape)
    returned = lax.all_to_all(served, ("sp", "dp"), split_axis=0, concat_axis=0, tiled=True)
    gathered = returned.reshape(experts * capacity, width)[target].reshape(tok_rows, TOPK, width)
    combined = jnp.sum(
        route_weight.reshape(tok_rows, TOPK, 1) * gathered.astype(jnp.float32), axis=1
    )
    mixed = (hidden_state.astype(jnp.float32) + scale_rows(combined, out_gain)).astype(jnp.bfloat16)
    return mixed.reshape(1, tok_rows, width)


def solution(mesh):
    in_specs = (
        P("dp", "sp", None),
        P("dp", "sp", None),
        P("dp", "sp", None),
        P("dp", "sp", None),
        P("dp", "sp", None),
        P(),
        P(),
        P(),
        P("dp", "sp", None),
        P(),
        P(),
        P("dp", "sp", None),
        P("dp", "sp", None),
        P(("sp", "dp"), None, None),
        P(("sp", "dp"), None, None),
        P(("sp", "dp"), None, None),
        P(),
    )
    out_specs = P("dp", "sp", None)
    return jax.shard_map(local, mesh=mesh, in_specs=in_specs, out_specs=out_specs, check_vma=False)
```

profile of v0, /device:TPU:0, one launch (start us, length us, event | category | flops | bytes accessed | tf_op | source)
XLA Modules:
  0.0 188.7 jit_solution(12045735491055822639)
XLA Ops:
  0.0 0.9 copy.25
  1.2 0.7 broadcast_multiply_fusion
  1.9 0.8 copy.21
  2.7 0.8 copy.22
  3.5 1.0 copy-done.3
  4.6 0.9 copy-done.4
  5.5 0.9 copy-done.5
  6.5 0.7 copy-done.8
  7.1 9.0 %block.1 = (bf16[8,64,384]{2,1,0:T(8,128)(2,1)S(1)}, f32[128,2048]{1,0:T(8,128)S(1)}, bf16[16,128,64]{2,1,0:T(8,128)(2,1)S(1)}) custom-call(bf16[128,1024]{1,0:T(8,128)(2,1)S(1)} %bitcast.53, bf16[128,1024]{1,0:T(8,128)(2,1)S(1)} %bitcast.54, bf16[128,2048]{1,0:T(8,128)(2,1)S(1)} %bitcast.52, bf16[128,16]{1,0:T(8,128)(2,1)S(1)} %bitcast.55, ...), custom_call_target="tpu_custom_call" | custom-call | tf_op jit(solution)/shard_map/block/pallas_call | solution.py:213
  16.1 3.4 %copy-done.1 = bf16[2048,2048]{1,0:T(8,128)(2,1)S(1)} copy-done((bf16[2048,2048]{1,0:T(8,128)(2,1)S(1)}, bf16[2048,2048]{1,0:T(8,128)(2,1)}, u32[]{:S(2)}) %copy-start.1) | copy-done | bytes 8388632
  19.5 1.0 copy-done.2
  20.5 0.7 copy-done.6
  21.2 0.7 copy-done.7
  21.9 0.7 copy-done.9
  22.6 25.0 %state.1 = (bf16[128,2048]{1,0:T(8,128)(2,1)S(1)}, bf16[128,2048]{1,0:T(8,128)(2,1)S(1)}) custom-call(bf16[8,64,384]{2,1,0:T(8,128)(2,1)S(1)} %get-tuple-element.10.ab_ref, f32[128,2048]{1,0:T(8,128)S(1)} %get-tuple-element.11.o_ref, bf16[16,128,64]{2,1,0:T(8,128)(2,1)S(1)} %get-tuple-element.12.qe_ref, f32[1,128]{1,0:T(1,128)S(1)} %bitcast.60, ...), custom_call_target="tpu_custom_call" | custom-call | tf_op jit(solution)/shard_map/state/pallas_call | solution.py:225
  47.6 1.6 broadcast_in_dim.5
  49.2 2.3 %reshape.116 = bf16[256,2048]{1,0:T(8,128)(2,1)} reshape(bf16[128,2,2048]{2,1,0:T(2,128)(2,1)} %broadcast_in_dim.5) | data formatting | bytes 2097152 | tf_op jit(solution)/shard_map/reshape | solution.py:254
  51.4 0.6 reduce-window.6
  52.0 0.2 slice_reduce_fusion
  52.4 0.1 mul.59
  52.6 4.4 %scatter_custom_fusion = bf16[512,2048]{1,0:T(8,128)(2,1)} fusion(s32[256]{0:T(256)S(1)} %bitcast.65, bf16[256,2048]{1,0:T(8,128)(2,1)} %reshape.116, bf16[]{:T(256)} %constant.9.clone.1), kind=kCustom, calls=%fused_computation.13 | custom fusion | bytes 2097664 | tf_op jit(solution)/shard_map/scatter | solution.py:255
  57.1 54.5 %all_to_all.10 = bf16[32,16,2048]{2,1,0:T(8,128)(2,1)S(1)} all-to-all(bf16[32,16,2048]{2,1,0:T(8,128)(2,1)} %bitcast.61), channel_id=1, replica_groups=mesh['sp'=8,'dp'=4] {'sp','dp'}, dimensions={0} | all-to-all | bytes 4194304 | tf_op jit(solution)/shard_map/all_to_all | solution.py:256
  111.6 1.3 copy-done.10
  112.9 2.2 %fusion.3 = f32[512,512]{1,0:T(8,128)} fusion(bf16[512,2048]{1,0:T(8,128)(2,1)S(1)} %bitcast.63, bf16[1,2048,512]{2,1,0:T(8,128)(2,1)S(1)} %copy-done.13), kind=kOutput, calls=%fused_computation.6 | convolution fusion | flops 1073741824 | bytes 5242880 | tf_op jit(solution)/shard_map/dot_general | solution.py:182
  115.1 6.3 %convolution_convert_fusion = bf16[512,2048]{1,0:T(8,128)(2,1)} fusion(bf16[1,512,2048]{2,1,0:T(8,128)(2,1)S(1)} %copy-done, bf16[512,2048]{1,0:T(8,128)(2,1)} %bitcast.64, bf16[1,2048,512]{2,1,0:T(8,128)(2,1)} %param.31, f32[512,512]{1,0:T(8,128)} %fusion.3), kind=kOutput, calls=%fused_computation.2 | convolution fusion | flops 2150105088 | bytes 9437184 | tf_op jit(solution)/shard_map/dot_general | solution.py:185
  121.4 4.0 %all-to-all-start.1 = ((bf16[32,16,2048]{2,1,0:T(8,128)(2,1)}), bf16[32,16,2048]{2,1,0:T(8,128)(2,1)}, u32[]{:S(2)}, u32[]{:S(2)}) async-start(bf16[32,16,2048]{2,1,0:T(8,128)(2,1)} %bitcast.62), calls=%async_computation.1 | async-start | bytes 4194304 | tf_op jit(solution)/shard_map/all_to_all | solution.py:266
  125.6 48.5 %all-to-all-done.1 = bf16[32,16,2048]{2,1,0:T(8,128)(2,1)} async-done(((bf16[32,16,2048]{2,1,0:T(8,128)(2,1)}), bf16[32,16,2048]{2,1,0:T(8,128)(2,1)}, u32[]{:S(2)}, u32[]{:S(2)}) %all-to-all-start.1) | async-done | bytes 2097184 | tf_op jit(solution)/shard_map/all_to_all | solution.py:266
  174.1 5.2 %gather_fusion = bf16[256,2048]{1,0:T(8,128)(2,1)} fusion(bf16[512,2048]{1,0:T(8,128)(2,1)} %bitcast.20, s32[1024]{0:T(1024)S(1)} %pad_clamp_fusion), kind=kCustom, calls=%fused_computation | custom fusion | bytes 2098176 | tf_op jit(solution)/shard_map/gather | solution.py:267
  179.3 3.4 %reshape.103 = f32[128,2,2048]{2,1,0:T(2,128)} reshape(bf16[256,2048]{1,0:T(8,128)(2,1)} %gather_fusion) | data formatting | bytes 3145728 | tf_op jit(solution)/shard_map/convert_element_type | solution.py:269
  182.7 4.8 %multiply_reduce_fusion = f32[128,2048]{1,0:T(8,128)S(1)} fusion(f32[128,2,2048]{2,1,0:T(2,128)} %reshape.103, f32[128,2]{1,0:T(8,128)S(1)} %copy.23), kind=kLoop, calls=%fused_computation.8 | loop fusion | flops 786432 | bytes 3146752 | tf_op jit(solution)/shard_map/reduce_sum | solution.py:268
  187.5 0.2 multiply_reduce_fusion.1
  187.7 1.0 fusion.15
  (29 shorter events, 0.7 us)
Async XLA Ops:
  0.0 115.1 %copy-start = (bf16[1,512,2048]{2,1,0:T(8,128)(2,1)S(1)}, bf16[1,512,2048]{2,1,0:T(8,128)(2,1)}, u32[]{:S(2)}) copy-start(bf16[1,512,2048]{2,1,0:T(8,128)(2,1)} %param.32) | copy-start | bytes 6291460
  3.5 1.0 copy-start.3
  4.6 0.9 copy-start.4
  5.5 0.9 copy-start.5
  6.5 0.7 copy-start.8
  16.1 3.4 %copy-start.1 = (bf16[2048,2048]{1,0:T(8,128)(2,1)S(1)}, bf16[2048,2048]{1,0:T(8,128)(2,1)}, u32[]{:S(2)}) copy-start(bf16[2048,2048]{1,0:T(8,128)(2,1)} %w_hbm.1) | copy-start | bytes 25165828
  19.5 1.0 copy-start.2
  20.5 0.7 copy-start.6
  21.2 0.7 copy-start.7
  21.9 0.7 copy-start.9
  57.1 55.8 %copy-start.13 = (bf16[1,2048,512]{2,1,0:T(8,128)(2,1)S(1)}, bf16[1,2048,512]{2,1,0:T(8,128)(2,1)}, u32[]{:S(2)}) copy-start(bf16[1,2048,512]{2,1,0:T(8,128)(2,1)} %param.30) | copy-start | bytes 6291460
  111.6 1.3 copy-start.10
  121.4 4.0 %copy-start.12 = (f32[1,128,2]{1,2,0:T(2,128)S(1)}, f32[1,128,2]{1,2,0:T(2,128)}, u32[]{:S(2)}) copy-start(f32[1,128,2]{1,2,0:T(2,128)} %param.29) | copy-start | bytes 3076
  121.4 52.7 %all-to-all-start.1 = ((bf16[32,16,2048]{2,1,0:T(8,128)(2,1)}), bf16[32,16,2048]{2,1,0:T(8,128)(2,1)}, u32[]{:S(2)}, u32[]{:S(2)}) async-start(bf16[32,16,2048]{2,1,0:T(8,128)(2,1)} %bitcast.62), calls=%async_computation.1 | async-start | bytes 4194304 | tf_op jit(solution)/shard_map/all_to_all | solution.py:266
  182.7 5.0 %copy-start.11 = (f32[2048]{0:T(1024)S(1)}, f32[2048]{0:T(1024)}, u32[]{:S(2)}) copy-start(f32[2048]{0:T(1024)} %param.33) | copy-start | bytes 24580
where the time goes:
time: 189 us
  blocking collectives  54.5 us (29%)
  waiting for transfers between devices  48.5 us (26%)
  Pallas kernels  34 us (18%)
  local copies, waits for them, and re-layouts  31.6 us (17%)
  matrix products  8.49 us (4%)
  other arithmetic  7.43 us (4%)
  starting transfers between devices  4.02 us (2%)
    all_to_all x1, blocking collectives, local(): lax.all_to_all(outgoing.reshape(experts, capacity, width), ('sp', 'dp'),...  54.5 us
    all_to_all x1, waiting for transfers between devices, local(): lax.all_to_all(served, ('sp', 'dp'), split_axis=0, concat_axis=0, tiled=T...  48.5 us
    pallas_call x1, Pallas kernels, local(): pl.pallas_call(functools.partial(state_kernel, groups, local_heads), out_...  25 us
    unnamed x31, local copies, waits for them, and re-layouts  13.9 us
    pallas_call x1, Pallas kernels, local(): pl.pallas_call(functools.partial(block_kernel, groups, local_heads), out_...  8.99 us
    dot_general x1, matrix products, expert_ffn(): jnp.dot(inner, down_weight, preferred_element_type=jnp.float32)  6.27 us
    gather x1, local copies, waits for them, and re-layouts, local(): returned.reshape(experts * capacity, width)[target]  5.2 us
    reduce_sum x1, other arithmetic, local(): jnp.sum(route_weight.reshape(tok_rows, TOPK, 1) * gathered.astype(jnp.flo...  4.81 us
  transfers between devices with their start and end apart: 1, of which 1 were waited for; matrix products, arithmetic and copies ran while one was open for 0% of the time, Pallas kernels for 0%

commit v1 on v0

--- a/solution.py
+++ b/solution.py
@@ -178,6 +178,122 @@
     normed_ref[...] = scale_rows(hidden.astype(jnp.float32), fg_ref[...]).astype(HALF)
 
 
+def flip(index, mask, bits):
+    result = 0
+    for bit in range(bits):
+        own = (index // (1 << bit)) % 2
+        other = (mask // (1 << bit)) % 2
+        result = result + (own + other - 2 * own * other) * (1 << bit)
+    return result
+
+
+def expert_kernel(
+    groups, members, capacity,
+    normed_ref, hidden_ref, route_ref, share_ref, gain_ref, gate_hbm, up_hbm, down_hbm,
+    mixed_ref,
+    outgoing, arrived, served, returned, gate_ref, up_ref, down_ref,
+    w_sems, own_sem, send1, recv1, send2, recv2,
+):
+    sp, dp = lax.axis_index("sp"), lax.axis_index("dp")
+    count = groups * members
+    sp_bits, dp_bits = groups.bit_length() - 1, members.bit_length() - 1
+    fetches = [
+        pltpu.make_async_copy(source, target, w_sems.at[i])
+        for i, (source, target) in enumerate(((gate_hbm, gate_ref), (up_hbm, up_ref), (down_hbm, down_ref)))
+    ]
+    for fetch in fetches:
+        fetch.start()
+
+    def masks(k):
+        mask = count - 1 - k
+        return mask // members, mask % members
+
+    def partner(k):
+        sp_mask, dp_mask = masks(k)
+        return {"sp": flip(sp, sp_mask, sp_bits), "dp": flip(dp, dp_mask, dp_bits)}
+
+    barrier = pltpu.get_barrier_semaphore()
+    for k in range(count - 1):
+        pl.semaphore_signal(barrier, inc=1, device_id=partner(k), device_id_type=MESH)
+
+    tokens = normed_ref.shape[0]
+    slots = count * capacity
+    names = lax.broadcasted_iota(jnp.int32, (tokens, count), 1)
+    first, second = route_ref[:, 0:1] == names, route_ref[:, 1:2] == names
+    both = first.astype(jnp.float32) + second.astype(jnp.float32)
+    rows = lax.broadcasted_iota(jnp.int32, (tokens, tokens), 0)
+    cols = lax.broadcasted_iota(jnp.int32, (tokens, tokens), 1)
+    before = dot((rows > cols).astype(HALF), both.astype(HALF))
+    places = (both * (before + 1.0)).astype(HALF)
+    share = first.astype(jnp.float32) * share_ref[:, 0:1] + second.astype(jnp.float32) * share_ref[:, 1:2]
+    share_high = share.astype(HALF)
+    share_low = (share - share_high.astype(jnp.float32)).astype(HALF)
+
+    def owner_of(slot):
+        sp_mask, dp_mask = masks(slot // capacity)
+        return flip(sp, sp_mask, sp_bits) * members + flip(dp, dp_mask, dp_bits)
+
+    down_slot = lax.broadcasted_iota(jnp.int32, (slots, count), 0)
+    spread_rows = (owner_of(down_slot) == lax.broadcasted_iota(jnp.int32, (slots, count), 1)).astype(HALF)
+    turn = (lax.broadcasted_iota(jnp.int32, (slots, tokens), 0) % capacity + 1).astype(jnp.float32)
+    pick = (dot(spread_rows, places, NT) == turn).astype(HALF)
+    normed = normed_ref[...]
+    width = normed.shape[1]
+    chunk = slots // 4 if slots % (4 * capacity) == 0 else slots
+    per = chunk // capacity
+    for at in range(0, slots, chunk):
+        block = dot(pick[at : at + chunk], normed).astype(HALF)
+        outgoing[at // capacity : at // capacity + per] = block.reshape(per, capacity, width)
+
+    def go(k):
+        return pltpu.make_async_remote_copy(
+            src_ref=outgoing.at[k], dst_ref=arrived.at[k],
+            send_sem=send1.at[k], recv_sem=recv1.at[k],
+            device_id=partner(k), device_id_type=MESH,
+        )
+
+    def back(k):
+        return pltpu.make_async_remote_copy(
+            src_ref=served.at[k], dst_ref=returned.at[k],
+            send_sem=send2.at[k], recv_sem=recv2.at[k],
+            device_id=partner(k), device_id_type=MESH,
+        )
+
+    pl.semaphore_wait(barrier, count - 1)
+    for k in range(count - 1):
+        go(k).start()
+    own = pltpu.make_async_copy(outgoing.at[count - 1], arrived.at[count - 1], own_sem)
+    own.start()
+    own.wait()
+    match = dot(places, spread_rows, NT) == (
+        lax.broadcasted_iota(jnp.int32, (tokens, slots), 1) % capacity + 1
+    ).astype(jnp.float32)
+    high = jnp.where(match, dot(share_high, spread_rows, NT), 0.0).astype(HALF)
+    low = jnp.where(match, dot(share_low, spread_rows, NT), 0.0).astype(HALF)
+    for fetch in fetches:
+        fetch.wait()
+    for at in range(0, count, per):
+        for k in range(at, min(at + per, count - 1)):
+            go(k).wait()
+        rows_in = arrived[at : at + per].reshape(chunk, width)
+        gate = dot(rows_in, gate_ref[...])
+        inner = (gate / (1.0 + jnp.exp(-gate)) * dot(rows_in, up_ref[...])).astype(HALF)
+        served[at : at + per] = dot(inner, down_ref[...]).astype(HALF).reshape(per, capacity, width)
+        for k in range(at, min(at + per, count - 1)):
+            back(k).start()
+    own = pltpu.make_async_copy(served.at[count - 1], returned.at[count - 1], own_sem)
+    own.start()
+    own.wait()
+    total = jnp.zeros((tokens, width), jnp.float32)
+    for at in range(0, count, per):
+        for k in range(at, min(at + per, count - 1)):
+            back(k).wait()
+        block = returned[at : at + per].reshape(chunk, width)
+        low_slot, high_slot = at * capacity, at * capacity + chunk
+        total = total + dot(high[:, low_slot:high_slot], block) + dot(low[:, low_slot:high_slot], block)
+    mixed_ref[...] = (hidden_ref[...].astype(jnp.float32) + scale_rows(total, gain_ref[...])).astype(HALF)
+
+
 def expert_ffn(rows_in, gate_weight, up_weight, down_weight):
     gate = jnp.dot(rows_in, gate_weight, preferred_element_type=jnp.float32)
     upward = jnp.dot(rows_in, up_weight, preferred_element_type=jnp.float32)
@@ -219,7 +335,7 @@
         ),
         in_specs=[VMEM] * 6,
         out_specs=(VMEM,) * 3,
-        compiler_params=pltpu.CompilerParams(vmem_limit_bytes=40 << 20),
+        compiler_params=pltpu.CompilerParams(vmem_limit_bytes=60 * 1024 * 1024),
         name="block",
     )(queries[0], keys[0], values[0], decay_in[0], mix_in[0], rates.reshape(1, head_count))
     hidden_state, normed = pl.pallas_call(
@@ -238,7 +354,7 @@
         ]
         + [pltpu.SemaphoreType.DMA((groups,))] * 4,
         compiler_params=pltpu.CompilerParams(
-            collective_id=0, has_side_effects=True, vmem_limit_bytes=40 << 20
+            collective_id=0, has_side_effects=True, vmem_limit_bytes=60 * 1024 * 1024
         ),
         name="state",
     )(
@@ -247,6 +363,33 @@
     )
     experts = lax.axis_size("sp") * lax.axis_size("dp")
     capacity = max(2, 2 * tok_rows * TOPK // experts)
+    members = lax.axis_size("dp")
+    if capacity % 16 == 0 and not (groups & (groups - 1)) and not (members & (members - 1)):
+        hidden_units = w_gate.shape[2]
+        block = pltpu.VMEM((experts, capacity, width), HALF)
+        mixed = pl.pallas_call(
+            functools.partial(expert_kernel, groups, members, capacity),
+            out_shape=jax.ShapeDtypeStruct((tok_rows, width), HALF),
+            in_specs=[VMEM] * 5 + [ANY] * 3,
+            out_specs=VMEM,
+            scratch_shapes=[
+                block, block, block, block,
+                pltpu.VMEM((width, hidden_units), HALF),
+                pltpu.VMEM((width, hidden_units), HALF),
+                pltpu.VMEM((hidden_units, width), HALF),
+                pltpu.SemaphoreType.DMA((3,)),
+                pltpu.SemaphoreType.DMA,
+            ]
+            + [pltpu.SemaphoreType.DMA((experts,))] * 4,
+            compiler_params=pltpu.CompilerParams(
+                collective_id=1, has_side_effects=True, vmem_limit_bytes=60 * 1024 * 1024
+            ),
+            name="experts",
+        )(
+            normed, hidden_state, route[0], route_weight[0], out_gain.reshape(1, width),
+            w_gate[0], w_up[0], w_down[0],
+        )
+        return mixed[None]
     route_ids = route.reshape(tok_rows * TOPK)
     matches = (route_ids[:, None] == jnp.arange(experts, dtype=jnp.int32)).astype(jnp.int32)
     slot_index = jnp.sum((jnp.cumsum(matches, axis=0) - 1) * matches, axis=-1)

time: 189 us -> 150 us (0.79)
  Pallas kernels: 34 us -> 143 us
  blocking collectives: 54.5 us -> 0 us
  waiting for transfers between devices: 48.5 us -> 0 us
  local copies, waits for them, and re-layouts: 31.6 us -> 6.15 us
  matrix products: 8.49 us -> 0 us
  other arithmetic: 7.43 us -> 0 us
  starting transfers between devices: 4.02 us -> 0 us
    pallas_call x0 -> x1, Pallas kernels: none -> 105 us  [local(): pl.pallas_call(functools.partial(expert_kernel, groups, members, capacity...]
    all_to_all x1 -> x0, blocking collectives: 54.5 us -> none  [local(): lax.all_to_all(outgoing.reshape(experts, capacity, width), ('sp', 'dp'),...]
    all_to_all x1 -> x0, waiting for transfers between devices: 48.5 us -> none  [local(): lax.all_to_all(served, ('sp', 'dp'), split_axis=0, concat_axis=0, tiled=T...]
    dot_general x2 -> x0, matrix products: 8.49 us -> none  [the longest x1 6.27 us: expert_ffn(): jnp.dot(inner, down_weight, preferred_element_type=jnp.float32)]
    unnamed x31 -> x9, local copies, waits for them, and re-layouts: 13.9 us -> 6.15 us
    gather x1 -> x0, local copies, waits for them, and re-layouts: 5.2 us -> none  [local(): returned.reshape(experts * capacity, width)[target]]
    reduce_sum x3 -> x0, other arithmetic: 5.06 us -> none  [the longest x1 4.81 us: local(): jnp.sum(route_weight.reshape(tok_rows, TOPK, 1) * gathered.astype(jnp.flo...]
    scatter x1 -> x0, local copies, waits for them, and re-layouts: 4.43 us -> none  [local(): jnp.zeros((experts * capacity, width), jnp.bfloat16).at[target].set(copies)]
  transfers between devices with their start and end apart: 1 -> 0, of which waited for: 1 -> 0; matrix products, arithmetic and copies ran while one was open for 0% -> 0% of each run, Pallas kernels for 0% -> 0%
where the time goes in v1:
time: 150 us
  Pallas kernels  143 us (95%)
  local copies, waits for them, and re-layouts  6.15 us (4%)
    pallas_call x1, Pallas kernels, local(): pl.pallas_call(functools.partial(expert_kernel, groups, members, capacity...  105 us
    pallas_call x1, Pallas kernels, local(): pl.pallas_call(functools.partial(state_kernel, groups, local_heads), out_...  26.9 us
    pallas_call x1, Pallas kernels, local(): pl.pallas_call(functools.partial(block_kernel, groups, local_heads), out_...  11.4 us
    unnamed x9, local copies, waits for them, and re-layouts  6.15 us

profile of v1, /device:TPU:0, one launch (start us, length us, event | category | flops | bytes accessed | tf_op | source)
XLA Modules:
  0.0 149.5 jit_solution(5464233521860065818)
XLA Ops:
  0.0 1.4 copy.18
  1.4 1.4 copy.19
  2.8 11.4 %block.1 = (bf16[8,64,384]{2,1,0:T(8,128)(2,1)}, f32[128,2048]{1,0:T(8,128)}, bf16[16,128,64]{2,1,0:T(8,128)(2,1)}) custom-call(bf16[128,1024]{1,0:T(8,128)(2,1)} %bitcast.25, bf16[128,1024]{1,0:T(8,128)(2,1)} %bitcast.26, bf16[128,2048]{1,0:T(8,128)(2,1)} %bitcast.22, bf16[128,16]{1,0:T(8,128)(2,1)} %bitcast.27, bf16[128,16]{1,0:T(8,128)(2,1)} %bitcast.28, ...), custom_call_target="tpu_custom_call" | custom-call | tf_op jit(solution)/shard_map/block/pallas_call | solution.py:329
  14.2 0.0 copy-start
  14.2 0.0 copy-start.1
  14.2 26.9 %state.1 = (bf16[128,2048]{1,0:T(8,128)(2,1)}, bf16[128,2048]{1,0:T(8,128)(2,1)}) custom-call(bf16[8,64,384]{2,1,0:T(8,128)(2,1)} %get-tuple-element.10.ab_ref, f32[128,2048]{1,0:T(8,128)} %get-tuple-element.11.o_ref, bf16[16,128,64]{2,1,0:T(8,128)(2,1)} %get-tuple-element.12.qe_ref, f32[1,128]{1,0:T(1,128)} %bitcast.33, bf16[2048,2048]{1,0:T(8,128)(2,1)} %w_hbm.1, ...), custom_call_target="tpu_custom_call" | custom-call | tf_op jit(solution)/shard_map/state/pallas_call | solution.py:341
  41.1 0.0 copy-done
  41.1 0.7 copy.20
  41.9 0.0 copy-done.1
  41.9 0.7 copy.21
  42.6 105.0 %experts.1 = bf16[128,2048]{1,0:T(8,128)(2,1)} custom-call(bf16[128,2048]{1,0:T(8,128)(2,1)} %get-tuple-element.13.normed_ref, bf16[128,2048]{1,0:T(8,128)(2,1)} %get-tuple-element.14.hidden_ref, s32[128,2]{1,0:T(8,128)} %bitcast.23, f32[128,2]{1,0:T(8,128)} %bitcast.24, f32[1,2048]{1,0:T(1,128)} %bitcast.29, bf16[2048,512]{1,0:T(8,128)(2,1)} %bitcast.17, ...), custom_call_target="tpu_custom_call" | custom-call | tf_op jit(solution)/shard_map/experts/pallas_call | solution.py:370
  147.6 1.9 %copy.23 = bf16[1,128,2048]{2,1,0:T(8,128)(2,1)} copy(bf16[1,128,2048]{2,1,0:T(8,128)(2,1)} %bitcast.20) | data formatting | bytes 1048576
Async XLA Ops:
  14.2 27.0 %copy-start = (s32[1,128,2]{1,2,0:T(2,128)S(1)}, s32[1,128,2]{1,2,0:T(2,128)}, u32[]{:S(2)}) copy-start(s32[1,128,2]{1,2,0:T(2,128)} %param.28) | copy-start | bytes 3076
  14.2 27.7 %copy-start.1 = (f32[1,128,2]{1,2,0:T(2,128)S(1)}, f32[1,128,2]{1,2,0:T(2,128)}, u32[]{:S(2)}) copy-start(f32[1,128,2]{1,2,0:T(2,128)} %param.29) | copy-start | bytes 3076

commit v2 on v1

--- a/solution.py
+++ b/solution.py
@@ -47,9 +47,9 @@
     strict = rows > cols
     decay = decay_ref[...].astype(jnp.float32)
     softplus = jnp.maximum(decay, 0.0) + jnp.log1p(jnp.exp(-jnp.abs(decay)))
-    log_decay = -rates_ref[...] * softplus
     beta = 1.0 / (1.0 + jnp.exp(-mix_ref[...].astype(jnp.float32)))
-    running = dot(lower.astype(jnp.float32), log_decay, NN, PRECISE)
+    beta = dot((rows == cols).astype(jnp.float32), beta, NT, PRECISE)
+    running = dot(lower.astype(jnp.float32), softplus, NT, PRECISE) * -rates_ref[...]
     spot_r = lax.broadcasted_iota(jnp.int32, (heads, heads), 0)
     spot_c = lax.broadcasted_iota(jnp.int32, (heads, heads), 1)
     running_t = dot((spot_r == spot_c).astype(jnp.float32), running, NT, PRECISE)
@@ -111,7 +111,7 @@
 
 
 def state_kernel(
-    groups, local_heads,
+    groups, local_heads, fused,
     ab_ref, o_ref, qe_ref, hg_ref, w_hbm, res_ref, mg_ref, fg_ref,
     hidden_ref, normed_ref,
     ab_in, s_out, s_in, att, w_ref,
@@ -119,11 +119,12 @@
 ):
     me = lax.axis_index("sp")
     fetch = pltpu.make_async_copy(w_hbm, w_ref, w_sem)
-    fetch.start()
-    barrier = pltpu.get_barrier_semaphore()
-    for step in range(1, groups):
-        pl.semaphore_signal(barrier, inc=1, device_id={"sp": lax.rem(me + step, groups)}, device_id_type=MESH)
-    pl.semaphore_wait(barrier, groups - 1)
+    if not fused:
+        fetch.start()
+        barrier = pltpu.get_barrier_semaphore()
+        for step in range(1, groups):
+            pl.semaphore_signal(barrier, inc=1, device_id={"sp": lax.rem(me + step, groups)}, device_id_type=MESH)
+        pl.semaphore_wait(barrier, groups - 1)
 
     def first_copy(step):
         peer = lax.rem(me + step, groups)
@@ -197,13 +198,6 @@
     sp, dp = lax.axis_index("sp"), lax.axis_index("dp")
     count = groups * members
     sp_bits, dp_bits = groups.bit_length() - 1, members.bit_length() - 1
-    fetches = [
-        pltpu.make_async_copy(source, target, w_sems.at[i])
-        for i, (source, target) in enumerate(((gate_hbm, gate_ref), (up_hbm, up_ref), (down_hbm, down_ref)))
-    ]
-    for fetch in fetches:
-        fetch.start()
-
     def masks(k):
         mask = count - 1 - k
         return mask // members, mask % members
@@ -212,22 +206,20 @@
         sp_mask, dp_mask = masks(k)
         return {"sp": flip(sp, sp_mask, sp_bits), "dp": flip(dp, dp_mask, dp_bits)}
 
-    barrier = pltpu.get_barrier_semaphore()
-    for k in range(count - 1):
-        pl.semaphore_signal(barrier, inc=1, device_id=partner(k), device_id_type=MESH)
-
     tokens = normed_ref.shape[0]
     slots = count * capacity
-    names = lax.broadcasted_iota(jnp.int32, (tokens, count), 1)
-    first, second = route_ref[:, 0:1] == names, route_ref[:, 1:2] == names
+    names = lax.broadcasted_iota(jnp.int32, (count, tokens), 0)
+    first, second = route_ref[0:1, :] == names, route_ref[1:2, :] == names
     both = first.astype(jnp.float32) + second.astype(jnp.float32)
     rows = lax.broadcasted_iota(jnp.int32, (tokens, tokens), 0)
     cols = lax.broadcasted_iota(jnp.int32, (tokens, tokens), 1)
-    before = dot((rows > cols).astype(HALF), both.astype(HALF))
-    places = (both * (before + 1.0)).astype(HALF)
-    share = first.astype(jnp.float32) * share_ref[:, 0:1] + second.astype(jnp.float32) * share_ref[:, 1:2]
-    share_high = share.astype(HALF)
-    share_low = (share - share_high.astype(jnp.float32)).astype(HALF)
+    before = dot(both.astype(HALF), (rows > cols).astype(HALF), NT)
+    places_t = (both * (before + 1.0)).astype(HALF)
+    share_t = first.astype(jnp.float32) * share_ref[0:1, :] + second.astype(jnp.float32) * share_ref[1:2, :]
+    high_t = share_t.astype(HALF)
+    low_t = (share_t - high_t.astype(jnp.float32)).astype(HALF)
+    turned = (rows == cols).astype(HALF)
+    places, share_high, share_low = (dot(turned, x, NT).astype(HALF) for x in (places_t, high_t, low_t))
 
     def owner_of(slot):
         sp_mask, dp_mask = masks(slot // capacity)
@@ -236,15 +228,11 @@
     down_slot = lax.broadcasted_iota(jnp.int32, (slots, count), 0)
     spread_rows = (owner_of(down_slot) == lax.broadcasted_iota(jnp.int32, (slots, count), 1)).astype(HALF)
     turn = (lax.broadcasted_iota(jnp.int32, (slots, tokens), 0) % capacity + 1).astype(jnp.float32)
-    pick = (dot(spread_rows, places, NT) == turn).astype(HALF)
+    pick = (dot(spread_rows, places_t) == turn).astype(HALF)
     normed = normed_ref[...]
     width = normed.shape[1]
     chunk = slots // 4 if slots % (4 * capacity) == 0 else slots
     per = chunk // capacity
-    for at in range(0, slots, chunk):
-        block = dot(pick[at : at + chunk], normed).astype(HALF)
-        outgoing[at // capacity : at // capacity + per] = block.reshape(per, capacity, width)
-
     def go(k):
         return pltpu.make_async_remote_copy(
             src_ref=outgoing.at[k], dst_ref=arrived.at[k],
@@ -259,9 +247,11 @@
             device_id=partner(k), device_id_type=MESH,
         )
 
-    pl.semaphore_wait(barrier, count - 1)
-    for k in range(count - 1):
-        go(k).start()
+    for at in range(0, slots, chunk):
+        block = dot(pick[at : at + chunk], normed).astype(HALF)
+        outgoing[at // capacity : at // capacity + per] = block.reshape(per, capacity, width)
+        for k in range(at // capacity, min(at // capacity + per, count - 1)):
+            go(k).start()
     own = pltpu.make_async_copy(outgoing.at[count - 1], arrived.at[count - 1], own_sem)
     own.start()
     own.wait()
@@ -270,8 +260,8 @@
     ).astype(jnp.float32)
     high = jnp.where(match, dot(share_high, spread_rows, NT), 0.0).astype(HALF)
     low = jnp.where(match, dot(share_low, spread_rows, NT), 0.0).astype(HALF)
-    for fetch in fetches:
-        fetch.wait()
+    for i, (source, target) in enumerate(((gate_hbm, gate_ref), (up_hbm, up_ref), (down_hbm, down_ref))):
+        pltpu.make_async_copy(source, target, w_sems.at[i]).wait()
     for at in range(0, count, per):
         for k in range(at, min(at + per, count - 1)):
             go(k).wait()
@@ -292,6 +282,45 @@
         low_slot, high_slot = at * capacity, at * capacity + chunk
         total = total + dot(high[:, low_slot:high_slot], block) + dot(low[:, low_slot:high_slot], block)
     mixed_ref[...] = (hidden_ref[...].astype(jnp.float32) + scale_rows(total, gain_ref[...])).astype(HALF)
+
+
+def layer_kernel(
+    groups, members, local_heads, capacity,
+    q_ref, k_ref, v_ref, decay_ref, mix_ref, rates_ref,
+    hg_ref, w_hbm, res_ref, mg_ref, fg_ref,
+    route_ref, share_ref, gain_ref, gate_hbm, up_hbm, down_hbm,
+    mixed_ref,
+    ab_ref, o_ref, qe_ref, hidden_ref, normed_ref,
+    ab_in, s_out, s_in, att, w_ref, w_sem, own_sem, send1, recv1, send2, recv2,
+    outgoing, arrived, served, returned, gate_ref, up_ref, down_ref,
+    w_sems, own_sem2, send3, recv3, send4, recv4,
+):
+    sp, dp = lax.axis_index("sp"), lax.axis_index("dp")
+    barrier = pltpu.get_barrier_semaphore()
+    for step in range(1, groups * members):
+        there = {"sp": lax.rem(sp + step // members, groups), "dp": lax.rem(dp + step % members, members)}
+        pl.semaphore_signal(barrier, inc=1, device_id=there, device_id_type=MESH)
+    pltpu.make_async_copy(w_hbm, w_ref, w_sem).start()
+    for i, (source, target) in enumerate(((gate_hbm, gate_ref), (up_hbm, up_ref), (down_hbm, down_ref))):
+        pltpu.make_async_copy(source, target, w_sems.at[i]).start()
+    block_kernel(
+        groups, local_heads, q_ref, k_ref, v_ref, decay_ref, mix_ref, rates_ref, ab_ref, o_ref, qe_ref
+    )
+    pl.semaphore_wait(barrier, groups * members - 1)
+    state_kernel(
+        groups, local_heads, True,
+        ab_ref, o_ref, qe_ref, hg_ref, w_hbm, res_ref, mg_ref, fg_ref,
+        hidden_ref, normed_ref,
+        ab_in, s_out, s_in, att, w_ref,
+        w_sem, own_sem, send1, recv1, send2, recv2,
+    )
+    expert_kernel(
+        groups, members, capacity,
+        normed_ref, hidden_ref, route_ref, share_ref, gain_ref, gate_hbm, up_hbm, down_hbm,
+        mixed_ref,
+        outgoing, arrived, served, returned, gate_ref, up_ref, down_ref,
+        w_sems, own_sem2, send3, recv3, send4, recv4,
+    )
 
 
 def expert_ffn(rows_in, gate_weight, up_weight, down_weight):
@@ -326,6 +355,53 @@
     local_heads = head_count // groups
     width = out_weight.shape[1]
     wide = pair_width(local_heads) + local_heads * DV
+    members = lax.axis_size("dp")
+    experts = groups * members
+    capacity = max(2, 2 * tok_rows * TOPK // experts)
+    if capacity % 16 == 0 and not (groups & (groups - 1)) and not (members & (members - 1)):
+        hidden_units = w_gate.shape[2]
+        block = pltpu.VMEM((experts, capacity, width), HALF)
+        states = pltpu.VMEM((groups, DK, local_heads * DV), HALF)
+        mixed = pl.pallas_call(
+            functools.partial(layer_kernel, groups, members, local_heads, capacity),
+            out_shape=jax.ShapeDtypeStruct((tok_rows, width), HALF),
+            in_specs=[VMEM] * 7 + [ANY] + [VMEM] * 6 + [ANY] * 3,
+            out_specs=VMEM,
+            scratch_shapes=[
+                pltpu.VMEM((groups, DK, wide), HALF),
+                pltpu.VMEM((tok_rows, head_count * DV), jnp.float32),
+                pltpu.VMEM((head_count, tok_rows, DK), HALF),
+                pltpu.VMEM((tok_rows, width), HALF),
+                pltpu.VMEM((tok_rows, width), HALF),
+                pltpu.VMEM((groups, DK, wide), HALF),
+                states, states,
+                pltpu.VMEM((tok_rows, head_count * DV), HALF),
+                pltpu.VMEM(out_weight.shape, HALF),
+                pltpu.SemaphoreType.DMA,
+                pltpu.SemaphoreType.DMA,
+            ]
+            + [pltpu.SemaphoreType.DMA((groups,))] * 4
+            + [
+                block, block, block, block,
+                pltpu.VMEM((width, hidden_units), HALF),
+                pltpu.VMEM((width, hidden_units), HALF),
+                pltpu.VMEM((hidden_units, width), HALF),
+                pltpu.SemaphoreType.DMA((3,)),
+                pltpu.SemaphoreType.DMA,
+            ]
+            + [pltpu.SemaphoreType.DMA((experts,))] * 4,
+            compiler_params=pltpu.CompilerParams(
+                collective_id=0, has_side_effects=True, vmem_limit_bytes=60 * 1024 * 1024
+            ),
+            name="layer",
+        )(
+            queries[0], keys[0], values[0], decay_in[0].T, mix_in[0].T, rates.reshape(1, head_count),
+            head_gain.reshape(1, DV), out_weight, residual[0],
+            mix_gain.reshape(1, width), ffn_gain.reshape(1, width),
+            route[0].T, route_weight[0].T, out_gain.reshape(1, width),
+            w_gate[0], w_up[0], w_down[0],
+        )
+        return mixed[None]
     pairs, partial, reads = pl.pallas_call(
         functools.partial(block_kernel, groups, local_heads),
         out_shape=(
@@ -337,9 +413,9 @@
         out_specs=(VMEM,) * 3,
         compiler_params=pltpu.CompilerParams(vmem_limit_bytes=60 * 1024 * 1024),
         name="block",
-    )(queries[0], keys[0], values[0], decay_in[0], mix_in[0], rates.reshape(1, head_count))
+    )(queries[0], keys[0], values[0], decay_in[0].T, mix_in[0].T, rates.reshape(1, head_count))
     hidden_state, normed = pl.pallas_call(
-        functools.partial(state_kernel, groups, local_heads),
+        functools.partial(state_kernel, groups, local_heads, False),
         out_shape=(jax.ShapeDtypeStruct((tok_rows, width), HALF),) * 2,
         in_specs=[VMEM] * 4 + [ANY] + [VMEM] * 3,
         out_specs=(VMEM,) * 2,
@@ -361,35 +437,6 @@
         pairs, partial, reads, head_gain.reshape(1, DV), out_weight, residual[0],
         mix_gain.reshape(1, width), ffn_gain.reshape(1, width),
     )
-    experts = lax.axis_size("sp") * lax.axis_size("dp")
-    capacity = max(2, 2 * tok_rows * TOPK // experts)
-    members = lax.axis_size("dp")
-    if capacity % 16 == 0 and not (groups & (groups - 1)) and not (members & (members - 1)):
-        hidden_units = w_gate.shape[2]
-        block = pltpu.VMEM((experts, capacity, width), HALF)
-        mixed = pl.pallas_call(
-            functools.partial(expert_kernel, groups, members, capacity),
-            out_shape=jax.ShapeDtypeStruct((tok_rows, width), HALF),
-            in_specs=[VMEM] * 5 + [ANY] * 3,
-            out_specs=VMEM,
-            scratch_shapes=[
-                block, block, block, block,
-                pltpu.VMEM((width, hidden_units), HALF),
-                pltpu.VMEM((width, hidden_units), HALF),
-                pltpu.VMEM((hidden_units, width), HALF),
-                pltpu.SemaphoreType.DMA((3,)),
-                pltpu.SemaphoreType.DMA,
-            ]
-            + [pltpu.SemaphoreType.DMA((experts,))] * 4,
-            compiler_params=pltpu.CompilerParams(
-                collective_id=1, has_side_effects=True, vmem_limit_bytes=60 * 1024 * 1024
-            ),
-            name="experts",
-        )(
-            normed, hidden_state, route[0], route_weight[0], out_gain.reshape(1, width),
-            w_gate[0], w_up[0], w_down[0],
-        )
-        return mixed[None]
     route_ids = route.reshape(tok_rows * TOPK)
     matches = (route_ids[:, None] == jnp.arange(experts, dtype=jnp.int32)).astype(jnp.int32)
     slot_index = jnp.sum((jnp.cumsum(matches, axis=0) - 1) * matches, axis=-1)

time: 150 us -> 132 us (0.88)
  Pallas kernels: 143 us -> 130 us
  local copies, waits for them, and re-layouts: 6.15 us -> 1.88 us
    pallas_call x3 -> x1, Pallas kernels: 143 us -> 130 us  [local(): pl.pallas_call(functools.partial(layer_kernel, groups, members, local_hea...]
    unnamed x9 -> x1, local copies, waits for them, and re-layouts: 6.15 us -> 1.88 us
where the time goes in v2:
time: 132 us
  Pallas kernels  130 us (98%)
  local copies, waits for them, and re-layouts  1.88 us (1%)
    pallas_call x1, Pallas kernels, local(): pl.pallas_call(functools.partial(layer_kernel, groups, members, local_hea...  130 us

profile of v2, /device:TPU:0, one launch (start us, length us, event | category | flops | bytes accessed | tf_op | source)
XLA Modules:
  0.0 131.9 jit_solution(7954380194504699288)
XLA Ops:
  0.0 130.0 %layer.1 = bf16[128,2048]{1,0:T(8,128)(2,1)} custom-call(bf16[128,1024]{1,0:T(8,128)(2,1)} %bitcast.31, bf16[128,1024]{1,0:T(8,128)(2,1)} %bitcast.32, bf16[128,2048]{1,0:T(8,128)(2,1)} %bitcast.29, bf16[16,128]{1,0:T(8,128)(2,1)} %bitcast.36, bf16[16,128]{1,0:T(8,128)(2,1)} %bitcast.37, f32[1,16]{1,0:T(1,128)} %bitcast.40, f32[1,128]{1,0:T(1,128)} %bitcast.41, ...), custom_call_target="tpu_custom_call" | custom-call | tf_op jit(solution)/shard_map/layer/pallas_call | solution.py:365
  130.0 1.9 %copy.19 = bf16[1,128,2048]{2,1,0:T(8,128)(2,1)} copy(bf16[1,128,2048]{2,1,0:T(8,128)(2,1)} %bitcast.28) | data formatting | bytes 1048576
